TPU v7x, 32 devices: a whole 2x2x4 slice. The times are simulated.
32 devices in a mesh: sp: 16 (over z, y, x), tp: 2 (over core).
Axes of the slice: x: 2, y: 2, z: 4, core: 2. Of those that a mesh axis runs over, the one named last changes fastest.
Arguments:
- tokens: bfloat16 [16384, 2048], P('sp', 'tp'), may hold values from -6 to 6
- norm_gain: float32 [2048], replicated, may hold values from 0.1 to 1.9
- w_conv_a: bfloat16 [2048, 1024], P('sp', 'tp'), may hold values from -0.125 to 0.125
- w_conv_gate: bfloat16 [2048, 1024], P('sp', 'tp'), may hold values from -0.125 to 0.125
- conv_weight: float32 [31, 1024], P(None, 'tp'), may hold values from -16 to 16
- conv_gain: float32 [1024], P('tp'), may hold values from 0.1 to 1.9
- w_query: bfloat16 [2048, 512], P('sp', 'tp'), may hold values from -0.125 to 0.125
- w_key: bfloat16 [2048, 512], P('sp', 'tp'), may hold values from -0.125 to 0.125
- w_value: bfloat16 [2048, 1024], P('sp', 'tp'), may hold values from -0.125 to 0.125
- w_outgate: bfloat16 [2048, 1024], P('sp', 'tp'), may hold values from -0.125 to 0.125
- w_decay: bfloat16 [2048, 512], P('sp', 'tp'), may hold values from -0.125 to 0.125
- decay_bias: float32 [512], P('tp'), may hold values from 0 to 12
- decay_extra: float32 [16384, 512], P('sp', 'tp'), may hold values from -2 to 0
- head_gain: float32 [128], replicated, may hold values from 0.1 to 1.9
- init_state: float32 [8, 64, 128], P('tp'), may hold values from -768 to 768
- w_out_conv: bfloat16 [1024, 2048], P('tp', 'sp'), may hold values from -0.125 to 0.125
- w_out_gla: bfloat16 [1024, 2048], P('tp', 'sp'), may hold values from -0.125 to 0.125
Outputs:
- mixed: bfloat16 [16384, 2048], P(('sp', 'tp'))
All inputs are finite; a program needn't handle non-finite values.
Results may differ from a plain program's by a relative error of at most 0.022.
Values may be sent and summed in bfloat16 or wider, within the bound.
A program may use at most 128 MiB of HBM per device.

v0:
```python
import jax
import jax.numpy as jnp
from jax import lax
from jax.sharding import PartitionSpec as P

D_CONV = 1024
HK = 64
HV = 128
BLOCK = 64
epsilon = 1e-06
gate_divisor = 16.0
highest_precision = lax.Precision.HIGHEST


def passed_along(value, axis, steps):
    count = lax.axis_size(axis)
    first, last = (max(0, -steps), min(count, count - steps))
    return lax.ppermute(value, axis, [(source, source + steps) for source in range(first, last)])


def entering(array, axis, join, neutral):
    place = lax.axis_index(axis)
    gathered = jax.tree.map(
        lambda a, kind: lax.all_gather(a.astype(kind), axis), array, (jnp.bfloat16, jnp.bfloat16)
    )
    state = jax.tree.map(lambda a, e: jnp.zeros_like(a) + jnp.asarray(e, a.dtype), array, neutral)

    def one(step, state):
        return join(
            state,
            jax.tree.map(
                lambda a, own: lax.dynamic_index_in_dim(a, step, 0, False).astype(own.dtype),
                gathered,
                array,
            ),
        )

    return lax.fori_loop(0, place, one, state)


def project(hidden, weight):
    return jnp.dot(hidden, weight, preferred_element_type=jnp.float32)


def rounded(values_f32):
    return lax.optimization_barrier(values_f32.astype(jnp.bfloat16)).astype(jnp.float32)


def fold_rows(normed, portions):
    return tuple((project(normed, portion) for portion in portions))


def conv_branch(conv_a, conv_gate, conv_weight, conv_gain):
    gated = (rounded(conv_a) * jax.nn.sigmoid(rounded(conv_gate))).astype(jnp.bfloat16)
    rim_rows = conv_weight.shape[0] - 1
    row_count = gated.shape[0]
    earlier = passed_along(gated[row_count - rim_rows :], "sp", 1)
    extended = jnp.concatenate([earlier, gated], axis=0).astype(jnp.float32)
    conv_sum = jnp.zeros(gated.shape, jnp.float32)
    for tap_index in range(conv_weight.shape[0]):
        conv_sum = (
            conv_sum + conv_weight[tap_index][None, :] * extended[tap_index : tap_index + row_count]
        )
    row_sums, row_squares = lax.psum(
        (jnp.sum(conv_sum, axis=1), jnp.sum(conv_sum * conv_sum, axis=1)), "tp"
    )
    mean_val = (row_sums / D_CONV)[:, None]
    square_mean = (row_squares / D_CONV)[:, None]
    conv_norm = (
        (conv_sum - mean_val) * lax.rsqrt(square_mean - mean_val * mean_val + epsilon) * conv_gain
    )
    return jax.nn.silu(conv_norm).astype(jnp.bfloat16)


def chain_step(earlier, later):
    return (earlier[0] * later[0], earlier[1] * later[0][:, :, None] + later[1])


def gla_branch(
    query, keys, values, out_gate, decay_pre, decay_bias, decay_extra, head_gain, init_state
):
    row_count = query.shape[0]
    local_heads = init_state.shape[0]
    blocks = row_count // BLOCK
    log_decay = jax.nn.log_sigmoid(decay_pre + decay_bias) / gate_divisor + decay_extra

    def to_heads(array, width):
        return array.reshape(blocks, BLOCK, local_heads, width).transpose(0, 2, 1, 3)

    query_heads = to_heads(rounded(query), HK) * HK ** (-0.5)
    key_heads = to_heads(rounded(keys), HK)
    value_heads = to_heads(rounded(values), HV)
    cum_log = jnp.cumsum(to_heads(log_decay, HK), axis=2)
    block_total = cum_log[:, :, -1:, :]
    query_decayed = query_heads * jnp.exp(cum_log)
    key_inverse = key_heads * jnp.exp(-cum_log)
    key_to_end = key_heads * jnp.exp(block_total - cum_log)
    causal = jnp.tril(jnp.ones((BLOCK, BLOCK), dtype=bool))
    scores = jnp.where(
        causal,
        jnp.einsum("nhik,nhjk->nhij", query_decayed, key_inverse, precision=highest_precision),
        0.0,
    )
    within = jnp.einsum("nhij,nhjv->nhiv", scores, value_heads, precision=highest_precision)

    def advance(state_current, block_items):
        query_block, key_block, value_block, decay_block = block_items
        carried_state = jnp.einsum(
            "yau,yub->yab", query_block, state_current, precision=highest_precision
        )
        state_following = state_current * decay_block[:, 0, :, None] + jnp.einsum(
            "tie,tis->tes", key_block, value_block, precision=highest_precision
        )
        return (state_following, carried_state)

    zero_state = jnp.zeros(init_state.shape, jnp.float32)
    local_end, carried_out = lax.scan(
        advance, zero_state, (query_decayed, key_to_end, value_heads, jnp.exp(block_total))
    )
    block_sums = block_total[:, :, 0, :]
    device_log = jnp.sum(block_sums, axis=0)
    prefix_log = jnp.cumsum(block_sums, axis=0) - block_sums
    before_decay, before_state = entering(
        (jnp.exp(device_log), local_end),
        "sp",
        chain_step,
        (jnp.ones_like(device_log), jnp.zeros_like(local_end)),
    )
    state_entering = before_state + init_state * before_decay[:, :, None]
    query_since_beginning = query_decayed * jnp.exp(prefix_log)[:, :, None, :]
    incoming_state = jnp.einsum(
        "oltu,luf->oltf", query_since_beginning, state_entering, precision=highest_precision
    )
    attn = within + carried_out + incoming_state
    normal_attn = (
        attn * lax.rsqrt(jnp.mean(attn * attn, axis=-1, keepdims=True) + epsilon) * head_gain
    )
    normal_attn = normal_attn.transpose(0, 2, 1, 3).reshape(row_count, local_heads * HV)
    return (normal_attn * jax.nn.silu(rounded(out_gate))).astype(jnp.bfloat16)


def per_device(
    tokens,
    norm_gain,
    w_conv_a,
    w_conv_gate,
    conv_weight,
    conv_gain,
    w_query,
    w_key,
    w_value,
    w_outgate,
    w_decay,
    decay_bias,
    decay_extra,
    head_gain,
    init_state,
    w_out_conv,
    w_out_gla,
):
    features = lax.all_gather(tokens, "tp", axis=1, tiled=True)
    widened = features.astype(jnp.float32)
    normed = (
        widened
        * lax.rsqrt(jnp.mean(widened * widened, axis=-1, keepdims=True) + epsilon)
        * norm_gain
    ).astype(jnp.bfloat16)
    projected = fold_rows(
        normed,
        (
            lax.all_gather(w_conv_a, "sp", axis=0, tiled=True),
            lax.all_gather(w_conv_gate, "sp", axis=0, tiled=True),
            lax.all_gather(w_query, "sp", axis=0, tiled=True),
            lax.all_gather(w_key, "sp", axis=0, tiled=True),
            lax.all_gather(w_value, "sp", axis=0, tiled=True),
            lax.all_gather(w_outgate, "sp", axis=0, tiled=True),
            lax.all_gather(w_decay, "sp", axis=0, tiled=True),
        ),
    )
    conv_proj = projected[:2]
    conv_out = conv_branch(conv_proj[0], conv_proj[1], conv_weight, conv_gain)
    gla_proj = projected[2:]
    gla_out = gla_branch(
        gla_proj[0],
        gla_proj[1],
        gla_proj[2],
        gla_proj[3],
        gla_proj[4],
        decay_bias,
        decay_extra,
        head_gain,
        init_state,
    )
    out_conv, out_gla = (
        lax.all_gather(w_out_conv, "sp", axis=1, tiled=True),
        lax.all_gather(w_out_gla, "sp", axis=1, tiled=True),
    )
    return lax.psum_scatter(
        (project(conv_out, out_conv) + project(gla_out, out_gla)).astype(jnp.bfloat16),
        "tp",
        scatter_dimension=0,
        tiled=True,
    )


def solution(mesh):
    placed = (
        P("sp", "tp"),
        P(),
        P("sp", "tp"),
        P("sp", "tp"),
        P(None, "tp"),
        P("tp"),
        P("sp", "tp"),
        P("sp", "tp"),
        P("sp", "tp"),
        P("sp", "tp"),
        P("sp", "tp"),
        P("tp"),
        P("sp", "tp"),
        P(),
        P("tp", None, None),
        P("tp", "sp"),
        P("tp", "sp"),
    )
    return jax.shard_map(
        per_device, mesh=mesh, in_specs=placed, out_specs=P(("sp", "tp"), None), check_vma=False
    )
```

profile of v0, /device:TPU:0, one launch (start us, length us, event | category | flops | bytes accessed | tf_op | source)
XLA Modules:
  0.0 656.3 jit_solution(9338845575659341172)
XLA Ops:
  12.8 12.5 %all-gather.15.cloned.1.call-done = bf16[1024,2048]{1,0:T(8,128)(2,1)} async-done(((bf16[1024,1024]{1,0:T(8,128)(2,1)}), bf16[1024,2048]{1,0:T(8,128)(2,1)}) %all-gather.15.cloned.1.call-update) | async-done | bytes 4194320 | tf_op jit(solution)/shard_map/all_gather | solution.py:161
  31.7 52.6 %all-gather.25.cloned.1.call-done = bf16[2048,256]{1,0:T(8,128)(2,1)} async-done(((bf16[128,256]{1,0:T(8,128)(2,1)}), bf16[2048,256]{1,0:T(8,128)(2,1)}) %all-gather.25.cloned.1.call-update) | async-done | bytes 1048592 | tf_op jit(solution)/shard_map/all_gather | solution.py:177
  84.4 4.2 fusion.67
  93.2 47.9 %all-gather.23.cloned.1.call-done = bf16[2048,256]{1,0:T(8,128)(2,1)} async-done(((bf16[128,256]{1,0:T(8,128)(2,1)}), bf16[2048,256]{1,0:T(8,128)(2,1)}) %all-gather.23.cloned.1.call-update) | async-done | bytes 1048592 | tf_op jit(solution)/shard_map/all_gather | solution.py:173
  147.1 50.5 %all-gather.27.cloned.1.call-done = bf16[2048,256]{1,0:T(8,128)(2,1)} async-done(((bf16[128,256]{1,0:T(8,128)(2,1)}), bf16[2048,256]{1,0:T(8,128)(2,1)}) %all-gather.27.cloned.1.call-update) | async-done | bytes 1048592 | tf_op jit(solution)/shard_map/all_gather | solution.py:174
  197.6 3.7 convolution_convert_fusion.4
  203.7 7.8 %bitcast_multiply_fusion.1 = (f32[16,4,64,64]{3,0,1,2:T(8,128)}, f32[16,4,64,64]{3,0,1,2:T(8,128)}, f32[16,4,64,64]{3,0,1,2:T(8,128)}, f32[16,4,64,64]{3,0,1,2:T(8,128)S(1)}) fusion(f32[16,4,64,64]{3,0,1,2:T(8,128)} %copy-done.1, f32[16,64,4,64]{3,2,1,0:T(4,128)} %reshape.76, f32[16,4,64]{2,0,1:T(8,128)S(1)} %get-tuple-element.156, ...), kind=kLoop, calls=%fused_computation.97 | loop fusion | flops 1572864 | bytes 7372800 | tf_op jit(solution)/shard_map/mul | solution.py:96
  214.1 45.4 %all-gather.29.cloned.1.call-done = bf16[2048,512]{1,0:T(8,128)(2,1)} async-done(((bf16[128,512]{1,0:T(8,128)(2,1)}), bf16[2048,512]{1,0:T(8,128)(2,1)}) %all-gather.29.cloned.1.call-update) | async-done | bytes 2097168 | tf_op jit(solution)/shard_map/all_gather | solution.py:175
  259.5 6.2 convolution_convert_fusion.1
  268.6 83.0 %while.26 = (s32[]{:T(128)}, f32[4,64,128]{2,1,0:T(8,128)S(1)}, f32[16,4,64,128]{3,2,1,0:T(8,128)}, f32[16,4,1,64]{3,0,1,2:T(8,128)}, f32[16,4,64,64]{3,0,1,2:T(...) while((s32[]{:T(128)}, f32[4,64,128]{2,1,0:T(8,128)S(1)}, ...), condition=%wide.region_7.8_spmd.clone, body=%wide.region_6.7_spmd.clone.sunk | while | flops 50462720 | bytes 1118832 | solution.py:117
  355.4 8.7 %fusion.54 = f32[16,4,64,64]{3,2,1,0:T(8,128)} fusion(f32[16,4,64,64]{3,0,1,2:T(8,128)} %get-tuple-element.152, f32[16,4,64,64]{3,0,1,2:T(8,128)S(1)} %get-tuple-element.155), kind=kOutput, calls=%fused_computation.101 | convolution fusion | flops 201326592 | bytes 3145728 | tf_op jit(solution)/shard_map/nhik,nhjk->nhij/dot_general | solution.py:101
  364.2 5.5 convolution_convert_fusion.3
  369.6 13.9 %all-gather.19.cloned.1.call-done = bf16[2048,512]{1,0:T(8,128)(2,1)} async-done(((bf16[128,512]{1,0:T(8,128)(2,1)}), bf16[2048,512]{1,0:T(8,128)(2,1)}) %all-gather.19.cloned.1.call-update) | async-done | bytes 2097168 | tf_op jit(solution)/shard_map/all_gather | solution.py:172
  383.5 5.2 convolution_convert_fusion.2
  392.5 53.0 %all-gather.31.cloned.1.call-done = bf16[2048,512]{1,0:T(8,128)(2,1)} async-done(((bf16[128,512]{1,0:T(8,128)(2,1)}), bf16[2048,512]{1,0:T(8,128)(2,1)}) %all-gather.31.cloned.1.call-update) | async-done | bytes 2097168 | tf_op jit(solution)/shard_map/all_gather | solution.py:176
  445.5 6.2 convolution_convert_fusion
  451.7 39.0 %all-gather.2 = bf16[16,4,64]{2,1,0:T(4,128)(2,1)S(1)} all-gather(bf16[1,4,64]{2,1,0:T(4,128)(2,1)S(1)} %fusion.85), channel_id=2, replica_groups=mesh['sp'=16,'tp'=2] {'sp'}, dimensions={0}, use_global_device_ids=true | all-gather | bytes 8704 | tf_op jit(solution)/shard_map/all_gather | solution.py:24
  491.0 9.5 %fusion.90 = (f32[1024]{0:T(1024)S(1)}, f32[1024]{0:T(1024)S(1)}, f32[1024,512]{1,0:T(8,128)}) fusion(f32[1054,512]{1,0:T(8,128)S(1)} %maximum_convert_fusion, f32[512]{0:T(512)S(1)} %bitcast.155, f32[512]{0:T(512)S(1)} %bitcast.156, f32[512]{0:T(512)S(1)} %bitcast.127, f32[512]{0:T(512)S(1)} %bitcast.128, f32[512]{0:T(512)S(1)} %bitcast.129, ...), kind=kLoop, calls=%fused_computation.160 | loop fusion | flops 33552384 | bytes 67180544 | tf_op jit(solution)/shard_map/reduce_sum | solution.py:65
  502.9 7.0 %all-gather.21.cloned.1.call-done = bf16[512,2048]{1,0:T(8,128)(2,1)} async-done(((bf16[512,128]{1,0:T(8,128)(2,1)}), bf16[512,2048]{1,0:T(8,128)(2,1)}) %all-gather.21.cloned.1.call-update) | async-done | bytes 2097168 | tf_op jit(solution)/shard_map/all_gather | solution.py:195
  509.9 8.3 %fusion.63 = f32[1024,2048]{1,0:T(8,128)} fusion(bf16[512,2048]{1,0:T(8,128)(2,1)} %all-gather.21.cloned.1.call-done, f32[1024,512]{1,0:T(8,128)} %get-tuple-element.151, f32[512]{0:T(512)S(1)} %copy-done.9, f32[1024]{0:T(1024)S(1)} %get-tuple-element.192, f32[1024]{0:T(1024)S(1)} %get-tuple-element.191), kind=kOutput, calls=%fused_computation.121 | convolution fusion | flops 2151677952 | bytes 12593152 | tf_op jit(solution)/shard_map/dot_general | solution.py:42
  518.2 47.6 %all-gather.35.cloned.1.call-done = bf16[64,64,128]{2,1,0:T(8,128)(2,1)} async-done(((bf16[4,64,128]{2,1,0:T(8,128)(2,1)}), bf16[64,64,128]{2,1,0:T(8,128)(2,1)}) %all-gather.35.cloned.1.call-update) | async-done | bytes 1048592 | tf_op jit(solution)/shard_map/all_gather | solution.py:24
  573.1 57.3 %all-gather.33.cloned.1.call-done = bf16[512,2048]{1,0:T(8,128)(2,1)} async-done(((bf16[512,128]{1,0:T(8,128)(2,1)}), bf16[512,2048]{1,0:T(8,128)(2,1)}) %all-gather.33.cloned.1.call-update) | async-done | bytes 2097168 | tf_op jit(solution)/shard_map/all_gather | solution.py:196
  630.4 8.5 %add_convert_fusion = bf16[1024,2048]{1,0:T(8,128)(2,1)} fusion(f32[1024,2048]{1,0:T(8,128)} %fusion.63, bf16[512,2048]{1,0:T(8,128)(2,1)} %all-gather.33.cloned.1.call-done, bf16[1024,512]{1,0:T(8,128)(2,1)S(1)} %copy-done.11, f32[128,8,4,128]{3,2,1,0:T(4,128)S(1)} %bitcast.123), kind=kOutput, calls=%fused_computation.24 | convolution fusion | flops 2155347968 | bytes 17825792 | tf_op jit(solution)/shard_map/dot_general | solution.py:42
  638.9 10.4 %reduce-scatter.2.cloned.1.call-done = bf16[512,2048]{1,0:T(8,128)(2,1)} async-done(((bf16[1024,2048]{1,0:T(8,128)(2,1)}), bf16[512,2048]{1,0:T(8,128)(2,1)}) %reduce-scatter.2.cloned.1.call-update) | async-done | bytes 2097168 | tf_op jit(solution)/shard_map/reduce_scatter | solution.py:198
  (166 shorter events, 130.8 us)
Async XLA Ops:
  6.5 18.8 %all-gather.15.cloned.1.call-start = ((), (), s32[]{:S(2)}) async-start(), calls=%async_computation.1 | async-start | bytes 6291456 | tf_op jit(solution)/shard_map/all_gather | solution.py:161
  7.3 77.1 %all-gather.25.cloned.1.call-start = ((), (), s32[]{:S(2)}) async-start(), calls=%async_computation.6 | async-start | bytes 1114112 | tf_op jit(solution)/shard_map/all_gather | solution.py:177
  8.0 133.1 %all-gather.23.cloned.1.call-start = ((), (), s32[]{:S(2)}) async-start(), calls=%async_computation.5 | async-start | bytes 1114112 | tf_op jit(solution)/shard_map/all_gather | solution.py:173
  8.7 188.9 %all-gather.27.cloned.1.call-start = ((), (), s32[]{:S(2)}) async-start(), calls=%async_computation.7 | async-start | bytes 1114112 | tf_op jit(solution)/shard_map/all_gather | solution.py:174
  9.3 250.2 %all-gather.29.cloned.1.call-start = ((), (), s32[]{:S(2)}) async-start(), calls=%async_computation.8 | async-start | bytes 2228224 | tf_op jit(solution)/shard_map/all_gather | solution.py:175
  9.9 354.3 %all-gather.17.cloned.1.call-start = ((), (), s32[]{:S(2)}) async-start(), calls=%async_computation.2 | async-start | bytes 2228224 | tf_op jit(solution)/shard_map/all_gather | solution.py:171
  10.5 373.0 %all-gather.19.cloned.1.call-start = ((), (), s32[]{:S(2)}) async-start(), calls=%async_computation.3 | async-start | bytes 2228224 | tf_op jit(solution)/shard_map/all_gather | solution.py:172
  11.2 434.3 %all-gather.31.cloned.1.call-start = ((), (), s32[]{:S(2)}) async-start(), calls=%async_computation.9 | async-start | bytes 2228224 | tf_op jit(solution)/shard_map/all_gather | solution.py:176
  12.0 497.9 %all-gather.21.cloned.1.call-start = ((), (), s32[]{:S(2)}) async-start(), calls=%async_computation.4 | async-start | bytes 2228224 | tf_op jit(solution)/shard_map/all_gather | solution.py:195
  12.7 553.1 %all-gather.35.cloned.1.call-start = ((), (), s32[]{:S(2)}) async-start(), calls=%async_computation.12 | async-start | bytes 1114112 | tf_op jit(solution)/shard_map/all_gather | solution.py:24
  12.8 15.8 %copy-start.6 = (f32[2048]{0:T(1024)S(1)}, f32[2048]{0:T(1024)}, u32[]{:S(2)}) copy-start(f32[2048]{0:T(1024)} %param.22) | copy-start | bytes 24580
  25.3 3.4 copy-start
  28.7 55.6 %copy-start.8 = (f32[1024,256]{1,0:T(8,128)S(1)}, f32[1024,256]{1,0:T(8,128)}, u32[]{:S(2)}) copy-start(f32[1024,256]{1,0:T(8,128)} %param.33) | copy-start | bytes 3145732
  28.7 55.6 %copy-start.10 = (f32[256]{0:T(256)S(1)}, f32[256]{0:T(256)}, u32[]{:S(2)}) copy-start(f32[256]{0:T(256)} %param.32) | copy-start | bytes 3076
  352.3 278.1 %all-gather.33.cloned.1.call-start = ((), (), s32[]{:S(2)}) async-start(), calls=%async_computation.10 | async-start | bytes 2228224 | tf_op jit(solution)/shard_map/all_gather | solution.py:196
  353.0 296.3 %reduce-scatter.2.cloned.1.call-start = ((), (), s32[]{:S(2)}) async-start(), calls=%async_computation.11 | async-start | bytes 6291456 | tf_op jit(solution)/shard_map/reduce_scatter | solution.py:198
  389.3 101.3 %collective-permute-start = (bf16[30,512]{1,0:T(8,128)(2,1)S(1)}, bf16[30,512]{1,0:T(8,128)(2,1)S(1)}, u32[]{:S(2)}, u32[]{:S(2)}) collective-permute-start(bf16[30,512]{1,0:T(8,128)(2,1)S(1)} %slice.256), channel_id=1, source_target_pairs={{0,2},{2,4},{4,6},{6,8},{8,10},{10,12},{12,14},{14,16},{16,18},{18... | collective-permute-start | bytes 92168 | tf_op jit(solution)/shard_map/ppermute | solution.py:18
  491.0 19.0 %copy-start.9 = (f32[512]{0:T(512)S(1)}, f32[512]{0:T(512)}, u32[]{:S(2)}) copy-start(f32[512]{0:T(512)} %param.26) | copy-start | bytes 6148
  509.9 56.0 %copy-start.2 = (f32[16,4,64,64]{3,0,1,2:T(8,128)S(1)}, f32[16,4,64,64]{3,0,1,2:T(8,128)}, u32[]{:S(2)}) copy-start(f32[16,4,64,64]{3,0,1,2:T(8,128)} %get-tuple-element.154) | copy-start | bytes 3145732
  518.2 47.7 %copy-start.5 = (f32[4,64,128]{2,1,0:T(8,128)S(1)}, f32[4,64,128]{2,1,0:T(8,128)}, u32[]{:S(2)}) copy-start(f32[4,64,128]{2,1,0:T(8,128)} %param.35) | copy-start | bytes 393220
  565.9 3.1 copy-start.3
  565.9 3.1 copy-start.4
  569.0 1.9 copy-start.7
  571.6 58.7 %copy-start.11 = (bf16[1024,512]{1,0:T(8,128)(2,1)S(1)}, bf16[1024,512]{1,0:T(8,128)(2,1)}, u32[]{:S(2)}) copy-start(bf16[1024,512]{1,0:T(8,128)(2,1)} %convolution_convert_fusion) | copy-start | bytes 3145732
  (1 other events, 1.3 us)
Sparse Core Ops, SparseCore 0:
  8.9 16.3 all-gather.14
  28.1 56.2 all-gather.24
  87.1 53.9 all-gather.22
  143.7 53.9 all-gather.26
  200.3 59.2 all-gather.28
  262.1 59.2 all-gather.16
  324.2 59.2 all-gather.18
  386.3 59.1 all-gather.30
  448.2 61.6 all-gather.20
  512.5 53.2 all-gather.34
  568.5 61.7 all-gather.32
  639.0 10.2 reduce-scatter.1
where the time goes:
time: 663 us; the launch traced here: 656 us
  waiting for transfers between devices  405 us (61%)
  matrix products  113 us (17%)
  local copies, waits for them, and re-layouts  49.1 us (7%)
  blocking collectives  41.4 us (6%)
  other arithmetic  29.9 us (5%)
  between operations  14.1 us (2%)
    all_gather x1, waiting for transfers between devices, per_device(): lax.all_gather(w_out_gla, 'sp', axis=1, tiled=True)  57.3 us
    all_gather x1, waiting for transfers between devices, per_device(): lax.all_gather(w_outgate, 'sp', axis=0, tiled=True)  53 us
    all_gather x1, waiting for transfers between devices, per_device(): lax.all_gather(w_decay, 'sp', axis=0, tiled=True)  52.6 us
    dot_general x9, matrix products, project(): return jnp.dot(hidden, weight, preferred_element_type=jnp.float32)  51.5 us
    all_gather x1, waiting for transfers between devices, per_device(): lax.all_gather(w_key, 'sp', axis=0, tiled=True)  50.5 us
    all_gather x1, waiting for transfers between devices, per_device(): lax.all_gather(w_query, 'sp', axis=0, tiled=True)  47.9 us
    all_gather x1, waiting for transfers between devices, entering(): lax.all_gather(a.astype(kind), axis)  47.6 us
    all_gather x1, waiting for transfers between devices, per_device(): lax.all_gather(w_value, 'sp', axis=0, tiled=True)  45.4 us
  transfers between devices with their start and end apart: 13, of which 11 were waited for; matrix products, arithmetic and copies ran while one was open for 28% of the time, Pallas kernels for 0%

commit v1 on v0

--- a/solution.py
+++ b/solution.py
@@ -193,7 +193,7 @@
     )
     out_conv, out_gla = (
         lax.all_gather(w_out_conv, "sp", axis=1, tiled=True),
-        lax.all_gather(w_out_gla, "sp", axis=1, tiled=True),
+        jnp.concatenate(lax.all_gather(w_out_gla, "sp"), axis=1),
     )
     return lax.psum_scatter(
         (project(conv_out, out_conv) + project(gla_out, out_gla)).astype(jnp.bfloat16),

time: 663 us -> 681 us (1.027)
  waiting for transfers between devices: 405 us -> 421 us
    reduce_scatter x1, waiting for transfers between devices: 10.4 us -> 26.5 us  [per_device(): lax.psum_scatter((project(conv_out, out_conv) + project(gla_out, out_gla)...]
    all_gather x1, waiting for transfers between devices: 13.9 us -> 25.6 us  [per_device(): lax.all_gather(w_conv_gate, 'sp', axis=0, tiled=True)]
    all_gather x1, waiting for transfers between devices: 53 us -> 44.6 us  [per_device(): lax.all_gather(w_outgate, 'sp', axis=0, tiled=True)]
  transfers between devices with their start and end apart: 13 -> 13, of which waited for: 11 -> 11; matrix products, arithmetic and copies ran while one was open for 28% -> 26% of each run, Pallas kernels for 0% -> 0%
where the time goes in v1:
time: 681 us; the launch traced here: 674 us
  waiting for transfers between devices  421 us (62%)
  matrix products  108 us (16%)
  local copies, waits for them, and re-layouts  53.7 us (8%)
  blocking collectives  41.2 us (6%)
  other arithmetic  30.9 us (5%)
  between operations  14.7 us (2%)
    all_gather x1, waiting for transfers between devices, per_device(): lax.all_gather(w_out_gla, 'sp')  58.5 us
    all_gather x1, waiting for transfers between devices, per_device(): lax.all_gather(w_decay, 'sp', axis=0, tiled=True)  52.6 us
    all_gather x1, waiting for transfers between devices, per_device(): lax.all_gather(w_key, 'sp', axis=0, tiled=True)  50.5 us
    dot_general x9, matrix products, project(): return jnp.dot(hidden, weight, preferred_element_type=jnp.float32)  48.4 us
    all_gather x1, waiting for transfers between devices, entering(): lax.all_gather(a.astype(kind), axis)  47.7 us
    all_gather x1, waiting for transfers between devices, per_device(): lax.all_gather(w_query, 'sp', axis=0, tiled=True)  47.1 us
    all_gather x1, waiting for transfers between devices, per_device(): lax.all_gather(w_value, 'sp', axis=0, tiled=True)  45.5 us
    all_gather x1, waiting for transfers between devices, per_device(): lax.all_gather(w_outgate, 'sp', axis=0, tiled=True)  44.6 us
  transfers between devices with their start and end apart: 13, of which 11 were waited for; matrix products, arithmetic and copies ran while one was open for 26% of the time, Pallas kernels for 0%

profile of v1, /device:TPU:0, one launch (start us, length us, event | category | flops | bytes accessed | tf_op | source)
XLA Modules:
  0.0 673.7 jit_solution(12933443379926332688)
XLA Ops:
  14.7 58.5 %all-gather.36.cloned.1.call-done = bf16[8192,128]{1,0:T(8,128)(2,1)} async-done(((bf16[512,128]{1,0:T(8,128)(2,1)}), bf16[8192,128]{1,0:T(8,128)(2,1)}) %all-gather.36.cloned.1.call-update) | async-done | bytes 2097168 | tf_op jit(solution)/shard_map/all_gather | solution.py:196
  73.2 3.9 copy.69
  77.2 10.1 %all-gather.16.cloned.1.call-done = bf16[1024,2048]{1,0:T(8,128)(2,1)} async-done(((bf16[1024,1024]{1,0:T(8,128)(2,1)}), bf16[1024,2048]{1,0:T(8,128)(2,1)}) %all-gather.16.cloned.1.call-update) | async-done | bytes 4194320 | tf_op jit(solution)/shard_map/all_gather | solution.py:161
  93.8 52.6 %all-gather.26.cloned.1.call-done = bf16[2048,256]{1,0:T(8,128)(2,1)} async-done(((bf16[128,256]{1,0:T(8,128)(2,1)}), bf16[2048,256]{1,0:T(8,128)(2,1)}) %all-gather.26.cloned.1.call-update) | async-done | bytes 1048592 | tf_op jit(solution)/shard_map/all_gather | solution.py:177
  146.3 4.2 fusion.67
  155.8 47.1 %all-gather.24.cloned.1.call-done = bf16[2048,256]{1,0:T(8,128)(2,1)} async-done(((bf16[128,256]{1,0:T(8,128)(2,1)}), bf16[2048,256]{1,0:T(8,128)(2,1)}) %all-gather.24.cloned.1.call-update) | async-done | bytes 1048592 | tf_op jit(solution)/shard_map/all_gather | solution.py:173
  209.0 50.5 %all-gather.28.cloned.1.call-done = bf16[2048,256]{1,0:T(8,128)(2,1)} async-done(((bf16[128,256]{1,0:T(8,128)(2,1)}), bf16[2048,256]{1,0:T(8,128)(2,1)}) %all-gather.28.cloned.1.call-update) | async-done | bytes 1048592 | tf_op jit(solution)/shard_map/all_gather | solution.py:174
  265.4 7.8 %bitcast_multiply_fusion.1 = (f32[16,4,64,64]{3,0,1,2:T(8,128)}, f32[16,4,64,64]{3,0,1,2:T(8,128)}, f32[16,4,64,64]{3,0,1,2:T(8,128)}, f32[16,4,64,64]{3,0,1,2:T(8,128)S(1)}) fusion(f32[16,4,64,64]{3,0,1,2:T(8,128)} %copy-done.1, f32[16,64,4,64]{3,2,1,0:T(4,128)} %reshape.84, f32[16,4,64]{2,0,1:T(8,128)S(1)} %get-tuple-element.170, ...), kind=kLoop, calls=%fused_computation.95 | loop fusion | flops 1572864 | bytes 7372800 | tf_op jit(solution)/shard_map/mul | solution.py:96
  275.8 45.5 %all-gather.30.cloned.1.call-done = bf16[2048,512]{1,0:T(8,128)(2,1)} async-done(((bf16[128,512]{1,0:T(8,128)(2,1)}), bf16[2048,512]{1,0:T(8,128)(2,1)}) %all-gather.30.cloned.1.call-update) | async-done | bytes 2097168 | tf_op jit(solution)/shard_map/all_gather | solution.py:175
  321.3 6.1 convolution_convert_fusion.1
  330.4 83.1 %while.26 = (s32[]{:T(128)}, f32[4,64,128]{2,1,0:T(8,128)S(1)}, f32[16,4,64,128]{3,2,1,0:T(8,128)}, f32[16,4,1,64]{3,0,1,2:T(8,128)}, f32[16,4,64,64]{3,0,1,2:T(...) while((s32[]{:T(128)}, f32[4,64,128]{2,1,0:T(8,128)S(1)}, ...), condition=%wide.region_7.8_spmd.clone, body=%wide.region_6.7_spmd.clone.sunk | while | flops 50462720 | bytes 1118832 | solution.py:117
  413.5 6.2 convolution_convert_fusion.3
  419.8 25.6 %all-gather.20.cloned.1.call-done = bf16[2048,512]{1,0:T(8,128)(2,1)} async-done(((bf16[128,512]{1,0:T(8,128)(2,1)}), bf16[2048,512]{1,0:T(8,128)(2,1)}) %all-gather.20.cloned.1.call-update) | async-done | bytes 2097168 | tf_op jit(solution)/shard_map/all_gather | solution.py:172
  445.4 5.3 convolution_convert_fusion.2
  455.4 7.3 %fusion.54 = f32[16,4,64,64]{3,2,1,0:T(8,128)} fusion(f32[16,4,64,64]{3,0,1,2:T(8,128)S(1)} %copy-done.2, f32[16,4,64,64]{3,0,1,2:T(8,128)S(1)} %get-tuple-element.169), kind=kOutput, calls=%fused_computation.101 | convolution fusion | flops 201326592 | bytes 3145728 | tf_op jit(solution)/shard_map/nhik,nhjk->nhij/dot_general | solution.py:101
  462.8 44.6 %all-gather.32.cloned.1.call-done = bf16[2048,512]{1,0:T(8,128)(2,1)} async-done(((bf16[128,512]{1,0:T(8,128)(2,1)}), bf16[2048,512]{1,0:T(8,128)(2,1)}) %all-gather.32.cloned.1.call-update) | async-done | bytes 2097168 | tf_op jit(solution)/shard_map/all_gather | solution.py:176
  507.4 6.2 convolution_convert_fusion
  514.6 38.8 %all-gather.3 = bf16[16,4,64]{2,1,0:T(4,128)(2,1)S(1)} all-gather(bf16[1,4,64]{2,1,0:T(4,128)(2,1)S(1)} %fusion.85), channel_id=2, replica_groups=mesh['sp'=16,'tp'=2] {'sp'}, dimensions={0}, use_global_device_ids=true | all-gather | bytes 8704 | tf_op jit(solution)/shard_map/all_gather | solution.py:24
  554.0 9.7 %fusion.90 = (f32[1024]{0:T(1024)S(1)}, f32[1024]{0:T(1024)S(1)}, f32[1024,512]{1,0:T(8,128)}) fusion(f32[1054,512]{1,0:T(8,128)S(1)} %maximum_convert_fusion, f32[512]{0:T(512)S(1)} %bitcast.161, f32[512]{0:T(512)S(1)} %bitcast.162, f32[512]{0:T(512)S(1)} %bitcast.133, f32[512]{0:T(512)S(1)} %bitcast.134, f32[512]{0:T(512)S(1)} %bitcast.135, ...), kind=kLoop, calls=%fused_computation.160 | loop fusion | flops 33552384 | bytes 67180544 | tf_op jit(solution)/shard_map/reduce_sum | solution.py:65
  566.1 5.5 all-gather.22.cloned.1.call-done
  571.6 8.3 %fusion.63 = f32[1024,2048]{1,0:T(8,128)} fusion(bf16[512,2048]{1,0:T(8,128)(2,1)} %all-gather.22.cloned.1.call-done, f32[1024,512]{1,0:T(8,128)} %get-tuple-element.165, f32[512]{0:T(512)S(1)} %copy-done.45, f32[1024]{0:T(1024)S(1)} %get-tuple-element.206, f32[1024]{0:T(1024)S(1)} %get-tuple-element.205), kind=kOutput, calls=%fused_computation.121 | convolution fusion | flops 2151677952 | bytes 12593152 | tf_op jit(solution)/shard_map/dot_general | solution.py:42
  579.9 47.7 %all-gather.34.cloned.1.call-done = bf16[64,64,128]{2,1,0:T(8,128)(2,1)} async-done(((bf16[4,64,128]{2,1,0:T(8,128)(2,1)}), bf16[64,64,128]{2,1,0:T(8,128)(2,1)}) %all-gather.34.cloned.1.call-update) | async-done | bytes 1048592 | tf_op jit(solution)/shard_map/all_gather | solution.py:24
  635.6 4.5 add_convert_fusion
  640.1 26.5 %reduce-scatter.2.cloned.1.call-done = bf16[512,2048]{1,0:T(8,128)(2,1)} async-done(((bf16[1024,2048]{1,0:T(8,128)(2,1)}), bf16[512,2048]{1,0:T(8,128)(2,1)}) %reduce-scatter.2.cloned.1.call-update) | async-done | bytes 2097168 | tf_op jit(solution)/shard_map/reduce_scatter | solution.py:198
  (244 shorter events, 135.7 us)
Async XLA Ops:
  6.5 66.7 %all-gather.36.cloned.1.call-start = ((), (), s32[]{:S(2)}) async-start(), calls=%async_computation.12 | async-start | bytes 2228224 | tf_op jit(solution)/shard_map/all_gather | solution.py:196
  7.3 80.0 %all-gather.16.cloned.1.call-start = ((), (), s32[]{:S(2)}) async-start(), calls=%async_computation.1 | async-start | bytes 6291456 | tf_op jit(solution)/shard_map/all_gather | solution.py:161
  8.0 138.3 %all-gather.26.cloned.1.call-start = ((), (), s32[]{:S(2)}) async-start(), calls=%async_computation.6 | async-start | bytes 1114112 | tf_op jit(solution)/shard_map/all_gather | solution.py:177
  8.7 194.2 %all-gather.24.cloned.1.call-start = ((), (), s32[]{:S(2)}) async-start(), calls=%async_computation.5 | async-start | bytes 1114112 | tf_op jit(solution)/shard_map/all_gather | solution.py:173
  9.3 250.1 %all-gather.28.cloned.1.call-start = ((), (), s32[]{:S(2)}) async-start(), calls=%async_computation.7 | async-start | bytes 1114112 | tf_op jit(solution)/shard_map/all_gather | solution.py:174
  9.9 311.4 %all-gather.30.cloned.1.call-start = ((), (), s32[]{:S(2)}) async-start(), calls=%async_computation.8 | async-start | bytes 2228224 | tf_op jit(solution)/shard_map/all_gather | solution.py:175
  10.5 403.1 %all-gather.18.cloned.1.call-start = ((), (), s32[]{:S(2)}) async-start(), calls=%async_computation.2 | async-start | bytes 2228224 | tf_op jit(solution)/shard_map/all_gather | solution.py:171
  11.2 434.1 %all-gather.20.cloned.1.call-start = ((), (), s32[]{:S(2)}) async-start(), calls=%async_computation.3 | async-start | bytes 2228224 | tf_op jit(solution)/shard_map/all_gather | solution.py:172
  12.0 495.4 %all-gather.32.cloned.1.call-start = ((), (), s32[]{:S(2)}) async-start(), calls=%async_computation.9 | async-start | bytes 2228224 | tf_op jit(solution)/shard_map/all_gather | solution.py:176
  12.7 558.9 %all-gather.22.cloned.1.call-start = ((), (), s32[]{:S(2)}) async-start(), calls=%async_computation.4 | async-start | bytes 2228224 | tf_op jit(solution)/shard_map/all_gather | solution.py:195
  13.3 614.4 %all-gather.34.cloned.1.call-start = ((), (), s32[]{:S(2)}) async-start(), calls=%async_computation.11 | async-start | bytes 1114112 | tf_op jit(solution)/shard_map/all_gather | solution.py:24
  90.7 55.6 %copy-start.44 = (f32[1024,256]{1,0:T(8,128)S(1)}, f32[1024,256]{1,0:T(8,128)}, u32[]{:S(2)}) copy-start(f32[1024,256]{1,0:T(8,128)} %param.33) | copy-start | bytes 3145732
  90.7 55.6 %copy-start.46 = (f32[256]{0:T(256)S(1)}, f32[256]{0:T(256)}, u32[]{:S(2)}) copy-start(f32[256]{0:T(256)} %param.32) | copy-start | bytes 3076
  452.2 101.1 %collective-permute-start = (bf16[30,512]{1,0:T(8,128)(2,1)S(1)}, bf16[30,512]{1,0:T(8,128)(2,1)S(1)}, u32[]{:S(2)}, u32[]{:S(2)}) collective-permute-start(bf16[30,512]{1,0:T(8,128)(2,1)S(1)} %slice.256), channel_id=1, source_target_pairs={{0,2},{2,4},{4,6},{6,8},{8,10},{10,12},{12,14},{14,16},{16,18},{18... | collective-permute-start | bytes 92168 | tf_op jit(solution)/shard_map/ppermute | solution.py:18
  462.8 51.1 %copy-start.42 = (f32[4,64]{1,0:T(4,128)S(1)}, f32[4,64]{1,0:T(4,128)}, u32[]{:S(2)}) copy-start(f32[4,64]{1,0:T(4,128)} %get-tuple-element.172) | copy-start | bytes 3076
  462.8 90.6 %copy-start.6 = (bf16[1024,512]{1,0:T(8,128)(2,1)S(1)}, bf16[1024,512]{1,0:T(8,128)(2,1)}, u32[]{:S(2)}) copy-start(bf16[1024,512]{1,0:T(8,128)(2,1)} %copy-done.5) | copy-start | bytes 3145732
  513.6 40.1 %copy-start.17 = (f32[1,512]{1,0:T(1,128)S(1)}, f32[1,512]{1,0:T(1,128)}, u32[]{:S(2)}) copy-start(f32[1,512]{1,0:T(1,128)} %get-tuple-element.180) | copy-start | bytes 6148
  513.6 40.1 %copy-start.18 = (f32[1,512]{1,0:T(1,128)S(1)}, f32[1,512]{1,0:T(1,128)}, u32[]{:S(2)}) copy-start(f32[1,512]{1,0:T(1,128)} %get-tuple-element.181) | copy-start | bytes 6148
  513.6 40.1 %copy-start.19 = (f32[1,512]{1,0:T(1,128)S(1)}, f32[1,512]{1,0:T(1,128)}, u32[]{:S(2)}) copy-start(f32[1,512]{1,0:T(1,128)} %get-tuple-element.182) | copy-start | bytes 6148
  513.6 40.1 %copy-start.20 = (f32[1,512]{1,0:T(1,128)S(1)}, f32[1,512]{1,0:T(1,128)}, u32[]{:S(2)}) copy-start(f32[1,512]{1,0:T(1,128)} %get-tuple-element.183) | copy-start | bytes 6148
  513.6 40.1 %copy-start.21 = (f32[1,512]{1,0:T(1,128)S(1)}, f32[1,512]{1,0:T(1,128)}, u32[]{:S(2)}) copy-start(f32[1,512]{1,0:T(1,128)} %get-tuple-element.184) | copy-start | bytes 6148
  514.5 152.1 %reduce-scatter.2.cloned.1.call-start = ((), (), s32[]{:S(2)}) async-start(), calls=%async_computation.10 | async-start | bytes 6291456 | tf_op jit(solution)/shard_map/reduce_scatter | solution.py:198
  571.6 56.1 %copy-start.3 = (f32[16,4,64,64]{3,0,1,2:T(8,128)S(1)}, f32[16,4,64,64]{3,0,1,2:T(8,128)}, u32[]{:S(2)}) copy-start(f32[16,4,64,64]{3,0,1,2:T(8,128)} %get-tuple-element.168) | copy-start | bytes 3145732
  579.9 47.8 %copy-start.10 = (f32[4,64,128]{2,1,0:T(8,128)S(1)}, f32[4,64,128]{2,1,0:T(8,128)}, u32[]{:S(2)}) copy-start(f32[4,64,128]{2,1,0:T(8,128)} %param.35) | copy-start | bytes 393220
  (39 other events, 1040.1 us)
Sparse Core Ops, SparseCore 0:
  10.1 63.0 all-gather.35
  74.8 12.4 all-gather.15
  90.0 56.2 all-gather.25
  148.9 53.9 all-gather.23
  205.5 53.9 all-gather.27
  262.1 59.2 all-gather.29
  324.1 59.1 all-gather.17
  386.1 59.2 all-gather.19
  448.1 59.1 all-gather.31
  509.9 61.6 all-gather.21
  574.4 53.2 all-gather.33
  640.2 26.3 reduce-scatter.1
